TPU v7x, 32 devices: a whole 2x2x4 slice. The times are simulated.
32 devices in a mesh: ep: 16 (over z, y, x), tp: 2 (over core).
Axes of the slice: x: 2, y: 2, z: 4, core: 2. Of those that a mesh axis runs over, the one named last changes fastest.
Arguments:
- tokens: bfloat16 [256, 2048], P('ep'), may hold values from -6 to 6
- recurrent_state: float32 [256, 4, 128, 256], P('ep', 'tp'), may hold values from -6 to 6
- query_weight: bfloat16 [2048, 512], P(None, 'tp'), may hold values from -0.125 to 0.125
- key_weight: bfloat16 [2048, 512], P(None, 'tp'), may hold values from -0.125 to 0.125
- decay_weight: bfloat16 [2048, 512], P(None, 'tp'), may hold values from -0.5 to 0.5
- value_weight: bfloat16 [2048, 1024], P(None, 'tp'), may hold values from -0.125 to 0.125
- gate_weight: bfloat16 [2048, 1024], P(None, 'tp'), may hold values from -0.125 to 0.125
- head_gain: float32 [256], replicated, may hold values from 0.1 to 1.9
- output_weight: bfloat16 [1024, 2048], P('tp'), may hold values from -0.375 to 0.375
- norm_gain: float32 [2, 2048], replicated, may hold values from 0.1 to 1.9
- norm_bias: float32 [2, 2048], replicated, may hold values from -1.8 to 1.8
- group_router: bfloat16 [2048, 4], replicated, may hold values from -0.125 to 0.125
- router_weight: bfloat16 [2048, 32], replicated, may hold values from -0.125 to 0.125
- routes: int32 [256, 2], P('ep'), may hold values from 0 to 31, as said below
- expert_gate: bfloat16 [32, 2048, 256], P(('ep', 'tp')), may hold values from -0.125 to 0.125
- expert_up: bfloat16 [32, 2048, 256], P(('ep', 'tp')), may hold values from -0.125 to 0.125
- expert_down: bfloat16 [32, 256, 2048], P(('ep', 'tp')), may hold values from -1.5 to 1.5
Outputs:
- new_tokens: bfloat16 [256, 2048], P('ep', 'tp')
- new_state: float32 [256, 4, 128, 256], P('ep', 'tp')
Inputs may be any that keep to these rules, and one draw needn't show every extreme that they name: `routes`: each row names two different experts of one group (group g holds the experts g * 8 to g * 8 + 7). In the rows of one device each group is named by the same number of rows and no expert by more than 2 rows; some expert is named by exactly 2 rows of every device.
All inputs are finite; a program needn't handle non-finite values.
Results may differ from a plain program's by a relative error of at most 0.01.
Values may be sent and summed in bfloat16 or wider, within the bound.
No kernel may reach another device: no remote copies, remote signals or barrier semaphores. Data moves between devices by JAX's collectives and lax.ppermute only.
A program may use at most 128 MiB of HBM per device.

v0:
```python
import jax
import jax.numpy as jnp
from jax import lax
from jax.sharding import PartitionSpec as P

alpha_res = 2.0**0.5
eps_norm = 1e-05


def layer_normed(inputs, gain_row, bias_row):
    centered = inputs - jnp.mean(inputs, axis=-1, keepdims=True)
    spread = jnp.mean(centered * centered, axis=-1, keepdims=True)
    return centered * lax.rsqrt(spread + eps_norm) * gain_row + bias_row


def on_device(
    tokens,
    recurrent_state,
    query_weight,
    key_weight,
    decay_weight,
    value_weight,
    gate_weight,
    head_gain,
    output_weight,
    norm_gain,
    norm_bias,
    group_router,
    router_weight,
    routes,
    expert_gate,
    expert_up,
    expert_down,
):
    row_count, model_width = tokens.shape
    heads_here = recurrent_state.shape[1]
    key_dim = recurrent_state.shape[2]
    value_dim = recurrent_state.shape[3]

    def project(weight):
        return jnp.dot(tokens, weight, preferred_element_type=jnp.float32)

    queries = project(query_weight).reshape(row_count, heads_here, key_dim) * key_dim ** (-0.5)
    key_rows = project(key_weight).reshape(row_count, heads_here, key_dim)
    value_rows = project(value_weight).reshape(row_count, heads_here, value_dim)
    gate_rows = project(gate_weight)
    decay_rate = jnp.exp(jax.nn.log_sigmoid(project(decay_weight)) / 16.0).reshape(
        row_count, heads_here, key_dim
    )
    new_state = (
        decay_rate[..., None] * recurrent_state + key_rows[..., None] * value_rows[:, :, None, :]
    )
    readout = jnp.sum(queries[..., None] * new_state, axis=2)
    norm_scale = lax.rsqrt(jnp.mean(readout * readout, axis=-1, keepdims=True) + eps_norm)
    gated_rows = (
        (readout * norm_scale * head_gain).reshape(row_count, heads_here * value_dim)
        * jax.nn.silu(gate_rows)
    ).astype(jnp.bfloat16)
    partial_value = jnp.dot(gated_rows, output_weight, preferred_element_type=jnp.float32)
    mixed_sum = lax.psum(partial_value.astype(jnp.bfloat16), "tp").astype(jnp.float32)
    hidden = layer_normed(
        alpha_res * tokens.astype(jnp.float32) + mixed_sum, norm_gain[0], norm_bias[0]
    ).astype(jnp.bfloat16)
    group_count = group_router.shape[1]
    expert_count = router_weight.shape[1]
    per_group = expert_count // group_count
    top_count = routes.shape[1]
    group_logit = jnp.dot(hidden, group_router, preferred_element_type=jnp.float32)
    expert_logit = jnp.dot(hidden, router_weight, preferred_element_type=jnp.float32)
    chosen_group = routes[:, 0] // per_group
    group_hit = chosen_group[:, None] == jnp.arange(group_count, dtype=jnp.int32)[None, :]
    own_logit = jnp.sum(jnp.where(group_hit, group_logit, 0.0), axis=1, keepdims=True)
    group_share = 1.0 / jnp.sum(jnp.exp(group_logit - own_logit), axis=1)
    expert_hit = routes[:, :, None] == jnp.arange(expert_count, dtype=jnp.int32)[None, None, :]
    picked = jnp.sum(jnp.where(expert_hit, expert_logit[:, None, :], 0.0), axis=2)
    route_weight = group_share[:, None] * jax.nn.sigmoid(picked - picked[:, ::-1])
    ep_count = lax.axis_size("ep")
    tp_count = lax.axis_size("tp")
    pair_index = lax.axis_index("tp")
    local_experts = expert_gate.shape[0]
    capacity = 2 * max(1, row_count // expert_count)
    total_slots = expert_count * capacity
    own_slots = total_slots // tp_count
    flat_routes = routes.reshape(row_count * top_count)
    onehot = (flat_routes[:, None] == jnp.arange(expert_count, dtype=jnp.int32)[None, :]).astype(
        jnp.int32
    )
    earlier_count = jnp.sum((jnp.cumsum(onehot, axis=0) - onehot) * onehot, axis=1)
    slot_index = flat_routes * capacity + earlier_count
    pick_all = (slot_index[:, None] == jnp.arange(total_slots, dtype=jnp.int32)[None, :]).astype(
        jnp.bfloat16
    )
    pick_mine = lax.dynamic_slice_in_dim(
        pick_all.reshape(row_count * top_count, ep_count, tp_count, local_experts * capacity),
        pair_index,
        1,
        2,
    ).reshape(row_count * top_count, own_slots)
    outgoing = jnp.einsum(
        "rks,rd->sd",
        pick_mine.reshape(row_count, top_count, own_slots),
        hidden,
        preferred_element_type=jnp.float32,
    ).astype(jnp.bfloat16)
    outgoing = outgoing.reshape(ep_count, local_experts, capacity, model_width)
    col_width = model_width // tp_count
    col_start = pair_index * col_width
    arrived = lax.all_to_all(outgoing, "ep", split_axis=0, concat_axis=0, tiled=True)
    gate_part = jnp.einsum(
        "secd,edf->secf", arrived, expert_gate, preferred_element_type=jnp.float32
    )
    up_part = jnp.einsum("secd,edf->secf", arrived, expert_up, preferred_element_type=jnp.float32)
    activation = (jax.nn.silu(gate_part) * up_part).astype(jnp.bfloat16)
    results = jnp.einsum(
        "secf,efd->secd", activation, expert_down, preferred_element_type=jnp.float32
    ).astype(jnp.bfloat16)
    returned = lax.all_to_all(
        lax.all_to_all(results, "ep", split_axis=0, concat_axis=0, tiled=True),
        "tp",
        split_axis=3,
        concat_axis=1,
        tiled=True,
    )
    fetched = jnp.dot(
        pick_all, returned.reshape(total_slots, col_width), preferred_element_type=jnp.float32
    ).reshape(row_count, top_count, col_width)
    routed_sum = jnp.sum(route_weight[..., None] * fetched, axis=1)
    blended = (
        alpha_res * lax.dynamic_slice_in_dim(hidden, col_start, col_width, 1).astype(jnp.float32)
        + routed_sum
    )
    row_total, row_squares = lax.psum(
        (jnp.sum(blended, axis=1), jnp.sum(blended * blended, axis=1)), "tp"
    )
    row_mean = row_total / model_width
    spread = row_squares / model_width - row_mean * row_mean
    gain_part = lax.dynamic_slice_in_dim(norm_gain[1], col_start, col_width, 0)
    shift_part = lax.dynamic_slice_in_dim(norm_bias[1], col_start, col_width, 0)
    new_tokens = (
        (blended - row_mean[:, None]) * lax.rsqrt(spread[:, None] + eps_norm) * gain_part
        + shift_part
    ).astype(jnp.bfloat16)
    return (new_tokens, new_state)


def solution(mesh):
    in_specs = (
        P("ep", None),
        P("ep", "tp", None, None),
        P(None, "tp"),
        P(None, "tp"),
        P(None, "tp"),
        P(None, "tp"),
        P(None, "tp"),
        P(),
        P("tp", None),
        P(),
        P(),
        P(),
        P(),
        P("ep", None),
        P(("ep", "tp"), None, None),
        P(("ep", "tp"), None, None),
        P(("ep", "tp"), None, None),
    )
    out_specs = (P("ep", "tp"), P("ep", "tp", None, None))
    return jax.shard_map(
        on_device, mesh=mesh, in_specs=in_specs, out_specs=out_specs, check_vma=False
    )
```

profile of v0, /device:TPU:0, one launch (start us, length us, event | category | flops | bytes accessed | tf_op | source)
XLA Modules:
  0.0 94.1 jit_solution(932960176985230560)
XLA Ops:
  7.2 0.0 copy-start
  7.2 0.0 all-reduce.3.cloned.1.call-start
  7.2 1.7 %convolution_multiply_fusion.1 = f32[16,256]{1,0:T(8,128)S(1)} fusion(bf16[16,2048]{1,0:T(8,128)(2,1)} %param.17, bf16[2048,256]{1,0:T(8,128)(2,1)} %param.19), kind=kOutput, calls=%fused_computation.14 | convolution fusion | flops 16781312 | bytes 1130496 | tf_op jit(solution)/shard_map/dot_general | solution.py:41
  8.9 2.0 %fusion.42 = f32[16,512]{1,0:T(8,128)S(1)} fusion(bf16[16,2048]{1,0:T(8,128)(2,1)} %param.17, bf16[2048,512]{1,0:T(8,128)(2,1)} %param.22), kind=kOutput, calls=%fused_computation.83 | convolution fusion | flops 33554432 | bytes 2195456 | tf_op jit(solution)/shard_map/dot_general | solution.py:41
  11.0 0.2 fusion.41
  11.3 1.5 %fusion.25 = f32[16,256]{1,0:T(8,128)S(1)} fusion(bf16[16,2048]{1,0:T(8,128)(2,1)S(1)} %copy-done.1, bf16[2048,256]{1,0:T(8,128)(2,1)} %param.21), kind=kOutput, calls=%fused_computation.41 | convolution fusion | flops 16814080 | bytes 1130496 | tf_op jit(solution)/shard_map/dot_general | solution.py:41
  12.8 5.7 %multiply_reduce_fusion = (f32[16,2,256]{2,1,0:T(2,128)S(1)}, f32[16,2,128,256]{3,2,1,0:T(8,128)}) fusion(f32[16,2,128]{2,1,0:T(2,128)S(1)} %mul.188, f32[16,2,256]{2,1,0:T(2,128)S(1)} %mul.195, f32[16,2,128]{2,1,0:T(2,128)S(1)} %mul.193, f32[16,2,128,256]{3,2,1,0:T(8,128)} %param.18, f32[16,2,128]{2,1,0:T(2,128)S(1)} %mul.190), kind=kLoop, calls=%fused_computation | loop fusion | flops 5234688 | bytes 8503296 | tf_op jit(solution)/shard_map/reduce_sum | solution.py:53
  18.4 0.1 multiply_reduce_fusion.3
  18.6 0.1 broadcast_multiply_fusion
  18.7 3.0 %convolution_convert_fusion.2 = bf16[16,2048]{1,0:T(8,128)(2,1)} fusion(bf16[512,2048]{1,0:T(8,128)(2,1)S(1)} %copy-done, f32[16,512]{1,0:T(8,128)S(1)} %bitcast.96, f32[512]{0:T(512)S(1)} %bitcast.102, bf16[16,2048]{1,0:T(8,128)(2,1)S(1)} %copy-done.1, bf16[2048,512]{1,0:T(8,128)(2,1)} %param.23), kind=kOutput, calls=%fused_computation.5 | convolution fusion | flops 67198976 | bytes 4360192 | tf_op jit(solution)/shard_map/dot_general | solution.py:59
  21.7 0.0 all-reduce.3.cloned.1.call-update
  21.8 0.1 copy.52
  21.9 0.6 fusion.34
  22.4 0.1 eq.98
  22.5 0.1 fusion.27
  22.6 0.1 reduce_window_sum.11
  22.7 0.2 select_reduce_fusion
  22.9 0.1 reduce_sum.118
  23.0 0.8 fusion.10
  23.8 1.1 %reshape.146 = f32[16,2,32]{2,1,0:T(2,128)S(1)} reshape(f32[32,16,1,2]{3,1,0,2:T(8,128)} %fusion.10) | data formatting | bytes 8192 | tf_op jit(solution)/shard_map/rks,rd->sd/convert_element_type | solution.py:99
  24.9 0.1 copy.53
  25.0 0.6 multiply_add_fusion.3
  25.6 16.7 %all-reduce.3.cloned.1.call-done = bf16[16,2048]{1,0:T(8,128)(2,1)} async-done(((bf16[16,2048]{1,0:T(8,128)(2,1)}), bf16[16,2048]{1,0:T(8,128)(2,1)}) %all-reduce.3.cloned.1.call-update) | async-done | bytes 65552 | tf_op jit(solution)/shard_map/psum | solution.py:60
  42.4 1.0 %fusion.17 = f32[16]{0:T(128)S(1)} fusion(bf16[16,2048]{1,0:T(8,128)(2,1)} %all-reduce.3.cloned.1.call-done, bf16[16,2048]{1,0:T(8,128)(2,1)S(1)} %copy-done.1), kind=kLoop, calls=%fused_computation.27 | loop fusion | flops 163824 | bytes 131136 | tf_op jit(solution)/shard_map/reduce_sum | solution.py:11
  43.3 1.0 %multiply_reduce_fusion.1 = f32[16]{0:T(128)S(1)} fusion(bf16[16,2048]{1,0:T(8,128)(2,1)} %all-reduce.3.cloned.1.call-done, bf16[16,2048]{1,0:T(8,128)(2,1)S(1)} %copy-done.1, f32[16]{0:T(128)S(1)} %broadcast_multiply_fusion.2), kind=kLoop, calls=%fused_computation.23 | loop fusion | flops 229360 | bytes 131200 | tf_op jit(solution)/shard_map/reduce_sum | solution.py:12
  44.4 0.9 add_convert_fusion
  45.3 0.2 fusion.44
  45.5 0.7 reshape.139
  46.3 6.8 %all-to-all-start = ((bf16[16,1,2,2048]{3,2,1,0:T(2,128)(2,1)}), bf16[16,1,2,2048]{3,2,1,0:T(2,128)(2,1)S(1)}, u32[]{:S(2)}, u32[]{:S(2)}) async-start(bf16[16,1,2,2048]{3,2,1,0:T(2,128)(2,1)} %bitcast.4), calls=%async_computation | async-start | bytes 262144 | tf_op jit(solution)/shard_map/all_to_all | solution.py:108
  53.1 0.9 select_reduce_fusion.2
  54.0 0.1 fusion.43
  54.2 6.8 %all-to-all-done = bf16[16,1,2,2048]{3,2,1,0:T(2,128)(2,1)S(1)} async-done(((bf16[16,1,2,2048]{3,2,1,0:T(2,128)(2,1)}), bf16[16,1,2,2048]{3,2,1,0:T(2,128)(2,1)S(1)}, u32[]{:S(2)}, u32[]{:S(2)}) %all-to-all-start) | async-done | bytes 131104 | tf_op jit(solution)/shard_map/all_to_all | solution.py:108
  61.0 1.5 %convolution_bitcast_fusion.1 = f32[16,1,2,256]{3,0,2,1:T(8,128)S(1)} fusion(bf16[1,2048,256]{2,1,0:T(8,128)(2,1)} %param.31, bf16[16,1,2,2048]{3,2,1,0:T(2,128)(2,1)S(1)} %all-to-all-done), kind=kOutput, calls=%fused_computation.10 | convolution fusion | flops 33554432 | bytes 1212416 | tf_op jit(solution)/shard_map/secd,edf->secf/dot_general | solution.py:109
  62.5 2.0 %fusion = bf16[16,1,2,2048]{3,0,2,1:T(8,128)(2,1)S(1)} fusion(bf16[1,256,2048]{2,1,0:T(8,128)(2,1)S(1)} %copy-done.2, bf16[1,2048,256]{2,1,0:T(8,128)(2,1)} %param.32, bf16[16,1,2,2048]{3,2,1,0:T(2,128)(2,1)S(1)} %all-to-all-done, f32[16,1,2,256]{3,0,2,1:T(8,128)S(1)} %convolution_bitcast_fusion.1), kind=kOutput, calls=%fused_computation.4 | convolution fusion | flops 67223552 | bytes 2392064 | tf_op jit(solution)/shard_map/secf,efd->secd/dot_general | solution.py:114
  64.4 0.8 copy.56
  65.2 3.5 %all-to-all-start.1 = ((bf16[16,1,2,2048]{3,2,1,0:T(2,128)(2,1)}), bf16[16,1,2,2048]{3,2,1,0:T(2,128)(2,1)S(1)}, u32[]{:S(2)}, u32[]{:S(2)}) async-start(bf16[16,1,2,2048]{3,2,1,0:T(2,128)(2,1)} %copy.56), calls=%async_computation.1 | async-start | bytes 262144 | tf_op jit(solution)/shard_map/all_to_all | solution.py:118
  68.8 0.2 select_reduce_fusion.1
  69.0 7.6 %all-to-all-done.1 = bf16[16,1,2,2048]{3,2,1,0:T(2,128)(2,1)S(1)} async-done(((bf16[16,1,2,2048]{3,2,1,0:T(2,128)(2,1)}), bf16[16,1,2,2048]{3,2,1,0:T(2,128)(2,1)S(1)}, u32[]{:S(2)}, u32[]{:S(2)}) %all-to-all-start.1) | async-done | bytes 131104 | tf_op jit(solution)/shard_map/all_to_all | solution.py:118
  76.5 0.8 copy.57
  77.3 1.1 %reshape.152 = bf16[2,2,16384]{2,1,0:T(2,128)(2,1)S(1)} reshape(bf16[2048,1,2,16]{3,2,1,0:T(2,128)(2,1)S(1)} %bitcast.93) | data formatting | bytes 262144
  78.4 3.8 %all_to_all.25 = bf16[2,2,16384]{2,1,0:T(2,128)(2,1)S(1)} all-to-all(bf16[2,2,16384]{2,1,0:T(2,128)(2,1)S(1)} %reshape.152), channel_id=1, replica_groups=mesh['ep'=16,'tp'=2] {'tp'}, dimensions={0} | all-to-all | bytes 262144 | tf_op jit(solution)/shard_map/all_to_all | solution.py:117
  82.2 0.7 reshape.153
  82.9 0.8 copy.58
  83.7 0.1 reshape.150
  83.7 0.2 fusion.1
  84.0 0.1 fusion.32
  84.1 2.5 %all-reduce = (f32[16]{0:T(128)S(1)}, f32[16]{0:T(128)S(1)}) all-reduce(f32[16]{0:T(128)S(1)} %get-tuple-element.3, f32[16]{0:T(128)S(1)} %get-tuple-element.2), channel_id=1, replica_groups=mesh['ep'=16,'tp'=2] {'tp'}, use_global_device_ids=true, to_apply=%region_15.16 | all-reduce | flops 32 | bytes 256 | tf_op jit(solution)/shard_map/psum | solution.py:132
  86.6 0.7 add_convert_fusion.1
  (41 shorter events, 0.3 us)
Async XLA Ops:
  7.2 11.5 %copy-start = (bf16[512,2048]{1,0:T(8,128)(2,1)S(1)}, bf16[512,2048]{1,0:T(8,128)(2,1)}, u32[]{:S(2)}) copy-start(bf16[512,2048]{1,0:T(8,128)(2,1)} %param.25) | copy-start | bytes 6291460
  7.2 3.8 %copy-start.1 = (bf16[16,2048]{1,0:T(8,128)(2,1)S(1)}, bf16[16,2048]{1,0:T(8,128)(2,1)}, u32[]{:S(2)}) copy-start(bf16[16,2048]{1,0:T(8,128)(2,1)} %param.17) | copy-start | bytes 196612
  7.2 3.8 %copy-start.3 = (bf16[2048,256]{1,0:T(8,128)(2,1)S(1)}, bf16[2048,256]{1,0:T(8,128)(2,1)}, u32[]{:S(2)}) copy-start(bf16[2048,256]{1,0:T(8,128)(2,1)} %param.20) | copy-start | bytes 3145732
  7.2 35.2 %all-reduce.3.cloned.1.call-start = ((), (), s32[]{:S(2)}) async-start(), calls=%async_computation.3 | async-start | bytes 131072 | tf_op jit(solution)/shard_map/psum | solution.py:60
  12.8 5.9 %copy-start.9 = (f32[256]{0:T(256)S(1)}, f32[256]{0:T(256)}, u32[]{:S(2)}) copy-start(f32[256]{0:T(256)} %param.24) | copy-start | bytes 3076
  18.7 3.1 %copy-start.7 = (s32[16,2]{0,1:T(2,128)S(1)}, s32[16,2]{0,1:T(2,128)}, u32[]{:S(2)}) copy-start(s32[16,2]{0,1:T(2,128)} %param.30) | copy-start | bytes 388
  18.7 4.2 %copy-start.5 = (f32[2,2048]{1,0:T(2,128)S(1)}, f32[2,2048]{1,0:T(2,128)}, u32[]{:S(2)}) copy-start(f32[2,2048]{1,0:T(2,128)} %param.27) | copy-start | bytes 49156
  18.7 4.3 %copy-start.6 = (f32[2,2048]{1,0:T(2,128)S(1)}, f32[2,2048]{1,0:T(2,128)}, u32[]{:S(2)}) copy-start(f32[2,2048]{1,0:T(2,128)} %param.26) | copy-start | bytes 49156
  21.7 32.3 %copy-start.4 = (bf16[2048,32]{0,1:T(8,128)(2,1)S(1)}, bf16[2048,32]{0,1:T(8,128)(2,1)}, u32[]{:S(2)}) copy-start(bf16[2048,32]{0,1:T(8,128)(2,1)} %param.29) | copy-start | bytes 393220
  21.7 40.8 %copy-start.2 = (bf16[1,256,2048]{2,1,0:T(8,128)(2,1)S(1)}, bf16[1,256,2048]{2,1,0:T(8,128)(2,1)}, u32[]{:S(2)}) copy-start(bf16[1,256,2048]{2,1,0:T(8,128)(2,1)} %param.33) | copy-start | bytes 3145732
  46.3 14.7 %all-to-all-start = ((bf16[16,1,2,2048]{3,2,1,0:T(2,128)(2,1)}), bf16[16,1,2,2048]{3,2,1,0:T(2,128)(2,1)S(1)}, u32[]{:S(2)}, u32[]{:S(2)}) async-start(bf16[16,1,2,2048]{3,2,1,0:T(2,128)(2,1)} %bitcast.4), calls=%async_computation | async-start | bytes 262144 | tf_op jit(solution)/shard_map/all_to_all | solution.py:108
  65.2 11.3 %all-to-all-start.1 = ((bf16[16,1,2,2048]{3,2,1,0:T(2,128)(2,1)}), bf16[16,1,2,2048]{3,2,1,0:T(2,128)(2,1)S(1)}, u32[]{:S(2)}, u32[]{:S(2)}) async-start(bf16[16,1,2,2048]{3,2,1,0:T(2,128)(2,1)} %copy.56), calls=%async_computation.1 | async-start | bytes 262144 | tf_op jit(solution)/shard_map/all_to_all | solution.py:118
  77.3 6.5 %copy-start.8 = (s32[16,2]{0,1:T(2,128)S(1)}, s32[16,2]{0,1:T(2,128)}, u32[]{:S(2)}) copy-start(s32[16,2]{0,1:T(2,128)} %multiply_add_fusion.3) | copy-start | bytes 388
Sparse Core Ops, SparseCore 0:
  21.9 20.4 all-reduce.2
where the time goes:
time: 94.9 us; the launch traced here: 94.1 us
  waiting for transfers between devices  31.1 us (33%)
  between operations  14.4 us (15%)
  matrix products  13.3 us (14%)
  other arithmetic  12.1 us (13%)
  starting transfers between devices  10.4 us (11%)
  local copies, waits for them, and re-layouts  6.53 us (7%)
  blocking collectives  6.31 us (7%)
    psum x1, waiting for transfers between devices, on_device(): lax.psum(partial_value.astype(jnp.bfloat16), 'tp').astype(jnp.float32)  16.7 us
    all_to_all x1, waiting for transfers between devices, on_device(): lax.all_to_all(results, 'ep', split_axis=0, concat_axis=0, tiled=True)  7.57 us
    all_to_all x1, starting transfers between devices, on_device(): lax.all_to_all(outgoing, 'ep', split_axis=0, concat_axis=0, tiled=True)  6.83 us
    all_to_all x1, waiting for transfers between devices, on_device(): lax.all_to_all(outgoing, 'ep', split_axis=0, concat_axis=0, tiled=True)  6.8 us
    reduce_sum x1, other arithmetic, on_device(): readout = jnp.sum(queries[..., None] * new_state, axis=2)  5.65 us
    dot_general x4, matrix products, project(): return jnp.dot(tokens, weight, preferred_element_type=jnp.float32)  5.4 us
    all_to_all x1, blocking collectives, on_device(): lax.all_to_all(lax.all_to_all(results, 'ep', split_axis=0, concat_axis=0,...  3.84 us
    all_to_all x1, starting transfers between devices, on_device(): lax.all_to_all(results, 'ep', split_axis=0, concat_axis=0, tiled=True)  3.51 us
  transfers between devices with their start and end apart: 3, of which 3 were waited for; matrix products, arithmetic and copies ran while one was open for 5% of the time, Pallas kernels for 0%

commit v1 on v0

--- a/solution.py
+++ b/solution.py
@@ -114,12 +114,20 @@
     results = jnp.einsum(
         "secf,efd->secd", activation, expert_down, preferred_element_type=jnp.float32
     ).astype(jnp.bfloat16)
-    returned = lax.all_to_all(
-        lax.all_to_all(results, "ep", split_axis=0, concat_axis=0, tiled=True),
-        "tp",
-        split_axis=3,
-        concat_axis=1,
-        tiled=True,
+    returned = jnp.concatenate(
+        lax.all_to_all(
+            jnp.stack(
+                jnp.split(
+                    lax.all_to_all(results, "ep", split_axis=0, concat_axis=0, tiled=True),
+                    lax.axis_size("tp"),
+                    axis=3,
+                )
+            ),
+            "tp",
+            0,
+            0,
+        ),
+        axis=1,
     )
     fetched = jnp.dot(
         pick_all, returned.reshape(total_slots, col_width), preferred_element_type=jnp.float32

time: 94.9 us -> 92 us (0.969)
  local copies, waits for them, and re-layouts: 6.53 us -> 2.49 us
  waiting for transfers between devices: 31.1 us -> 33 us
  other arithmetic: 12.1 us -> 10.5 us
    psum x1, waiting for transfers between devices: 16.7 us -> 19.5 us  [on_device(): lax.psum(partial_value.astype(jnp.bfloat16), 'tp').astype(jnp.float32)]
    unnamed x26 -> x20, local copies, waits for them, and re-layouts: 1.93 us -> 0.15 us
    all_to_all x2 -> x0, local copies, waits for them, and re-layouts: 1.51 us -> none  [the longest x1 0.76 us: on_device(): lax.all_to_all(results, 'ep', split_axis=0, concat_axis=0, tiled=True)]
  transfers between devices with their start and end apart: 3 -> 3, of which waited for: 3 -> 3; matrix products, arithmetic and copies ran while one was open for 5% -> 3% of each run, Pallas kernels for 0% -> 0%
where the time goes in v1:
time: 92 us; the launch traced here: 91.2 us
  waiting for transfers between devices  33 us (36%)
  between operations  14.4 us (16%)
  matrix products  14.2 us (15%)
  other arithmetic  10.5 us (11%)
  starting transfers between devices  10.4 us (11%)
  blocking collectives  6.31 us (7%)
  local copies, waits for them, and re-layouts  2.49 us (3%)
    psum x1, waiting for transfers between devices, on_device(): lax.psum(partial_value.astype(jnp.bfloat16), 'tp').astype(jnp.float32)  19.5 us
    all_to_all x1, waiting for transfers between devices, on_device(): lax.all_to_all(results, 'ep', split_axis=0, concat_axis=0, tiled=True)  7.57 us
    all_to_all x1, starting transfers between devices, on_device(): lax.all_to_all(outgoing, 'ep', split_axis=0, concat_axis=0, tiled=True)  6.83 us
    all_to_all x1, waiting for transfers between devices, on_device(): lax.all_to_all(outgoing, 'ep', split_axis=0, concat_axis=0, tiled=True)  5.89 us
    reduce_sum x1, other arithmetic, on_device(): readout = jnp.sum(queries[..., None] * new_state, axis=2)  5.65 us
    dot_general x4, matrix products, project(): return jnp.dot(tokens, weight, preferred_element_type=jnp.float32)  5.4 us
    all_to_all x1, blocking collectives, on_device(): lax.all_to_all(jnp.stack(jnp.split(lax.all_to_all(results, 'ep', split_ax...  3.84 us
    all_to_all x1, starting transfers between devices, on_device(): lax.all_to_all(results, 'ep', split_axis=0, concat_axis=0, tiled=True)  3.51 us
  transfers between devices with their start and end apart: 3, of which 3 were waited for; matrix products, arithmetic and copies ran while one was open for 3% of the time, Pallas kernels for 0%

profile of v1, /device:TPU:0, one launch (start us, length us, event | category | flops | bytes accessed | tf_op | source)
XLA Modules:
  0.0 91.2 jit_solution(15945548360208319777)
XLA Ops:
  7.2 0.0 copy-start
  7.2 0.0 copy-start.1
  7.2 0.0 all-reduce.3.cloned.1.call-start
  7.2 1.7 %convolution_multiply_fusion.1 = f32[16,256]{1,0:T(8,128)S(1)} fusion(bf16[16,2048]{1,0:T(8,128)(2,1)} %param.17, bf16[2048,256]{1,0:T(8,128)(2,1)} %param.19), kind=kOutput, calls=%fused_computation.14 | convolution fusion | flops 16781312 | bytes 1130496 | tf_op jit(solution)/shard_map/dot_general | solution.py:41
  8.9 2.0 %fusion.42 = f32[16,512]{1,0:T(8,128)S(1)} fusion(bf16[16,2048]{1,0:T(8,128)(2,1)} %param.17, bf16[2048,512]{1,0:T(8,128)(2,1)} %param.22), kind=kOutput, calls=%fused_computation.86 | convolution fusion | flops 33554432 | bytes 2195456 | tf_op jit(solution)/shard_map/dot_general | solution.py:41
  11.0 0.2 fusion.41
  11.3 1.5 %fusion.25 = f32[16,256]{1,0:T(8,128)S(1)} fusion(bf16[16,2048]{1,0:T(8,128)(2,1)S(1)} %copy-done.1, bf16[2048,256]{1,0:T(8,128)(2,1)} %param.21), kind=kOutput, calls=%fused_computation.44 | convolution fusion | flops 16814080 | bytes 1130496 | tf_op jit(solution)/shard_map/dot_general | solution.py:41
  12.8 0.0 copy-start.7
  12.8 5.7 %multiply_reduce_fusion = (f32[16,2,256]{2,1,0:T(2,128)S(1)}, f32[16,2,128,256]{3,2,1,0:T(8,128)}) fusion(f32[16,2,128]{2,1,0:T(2,128)S(1)} %mul.188, f32[16,2,256]{2,1,0:T(2,128)S(1)} %mul.195, f32[16,2,128]{2,1,0:T(2,128)S(1)} %mul.193, f32[16,2,128,256]{3,2,1,0:T(8,128)} %param.18, f32[16,2,128]{2,1,0:T(2,128)S(1)} %mul.190), kind=kLoop, calls=%fused_computation | loop fusion | flops 5234688 | bytes 8503296 | tf_op jit(solution)/shard_map/reduce_sum | solution.py:53
  18.4 0.1 multiply_reduce_fusion.3
  18.6 0.1 broadcast_multiply_fusion
  18.7 0.0 copy-start.6
  18.7 3.0 %convolution_convert_fusion.2 = bf16[16,2048]{1,0:T(8,128)(2,1)} fusion(bf16[512,2048]{1,0:T(8,128)(2,1)S(1)} %copy-done, f32[16,512]{1,0:T(8,128)S(1)} %bitcast.97, f32[512]{0:T(512)S(1)} %bitcast.103, bf16[16,2048]{1,0:T(8,128)(2,1)S(1)} %copy-done.1, bf16[2048,512]{1,0:T(8,128)(2,1)} %param.23), kind=kOutput, calls=%fused_computation.5 | convolution fusion | flops 67198976 | bytes 4360192 | tf_op jit(solution)/shard_map/dot_general | solution.py:59
  21.7 0.0 all-reduce.3.cloned.1.call-update
  21.8 0.1 copy.51
  21.9 0.1 eq.98
  21.9 0.1 fusion.27
  22.0 0.1 reduce_window_sum.11
  22.1 0.2 select_reduce_fusion
  22.3 0.1 reduce_sum.118
  22.4 0.0 copy-done.4
  22.5 0.1 fusion.10
  22.6 0.2 reshape.145
  22.7 0.1 copy.52
  22.9 19.5 %all-reduce.3.cloned.1.call-done = bf16[16,2048]{1,0:T(8,128)(2,1)} async-done(((bf16[16,2048]{1,0:T(8,128)(2,1)}), bf16[16,2048]{1,0:T(8,128)(2,1)}) %all-reduce.3.cloned.1.call-update) | async-done | bytes 65552 | tf_op jit(solution)/shard_map/psum | solution.py:60
  42.3 1.0 %fusion.17 = f32[16]{0:T(128)S(1)} fusion(bf16[16,2048]{1,0:T(8,128)(2,1)} %all-reduce.3.cloned.1.call-done, bf16[16,2048]{1,0:T(8,128)(2,1)S(1)} %copy-done.1), kind=kLoop, calls=%fused_computation.28 | loop fusion | flops 163824 | bytes 131136 | tf_op jit(solution)/shard_map/reduce_sum | solution.py:11
  43.3 1.0 %multiply_reduce_fusion.1 = f32[16]{0:T(128)S(1)} fusion(bf16[16,2048]{1,0:T(8,128)(2,1)} %all-reduce.3.cloned.1.call-done, bf16[16,2048]{1,0:T(8,128)(2,1)S(1)} %copy-done.1, f32[16]{0:T(128)S(1)} %broadcast_multiply_fusion.2), kind=kLoop, calls=%fused_computation.24 | loop fusion | flops 229360 | bytes 131200 | tf_op jit(solution)/shard_map/reduce_sum | solution.py:12
  44.4 0.9 %add_convert_fusion = bf16[16,2048]{1,0:T(8,128)(2,1)S(1)} fusion(bf16[16,2048]{1,0:T(8,128)(2,1)} %all-reduce.3.cloned.1.call-done, bf16[16,2048]{1,0:T(8,128)(2,1)S(1)} %copy-done.1, f32[2048]{0:T(1024)S(1)} %bitcast.99, f32[2048]{0:T(1024)S(1)} %bitcast.100, f32[16]{0:T(128)S(1)} %add_rsqrt_fusion.2, f32[16]{0:T(128)S(1)} %broadcast_multiply_fusion.2), kind=kLoop, calls=%fused_computation.23 | loop fusion | flops 294912 | bytes 213120 | tf_op jit(solution)/shard_map/convert_element_type | solution.py:63
  45.3 0.2 fusion.44
  45.5 0.7 reshape.138
  46.3 6.8 %all-to-all-start = ((bf16[16,1,2,2048]{3,2,1,0:T(2,128)(2,1)}), bf16[16,1,2,2048]{3,2,1,0:T(2,128)(2,1)S(1)}, u32[]{:S(2)}, u32[]{:S(2)}) async-start(bf16[16,1,2,2048]{3,2,1,0:T(2,128)(2,1)} %bitcast.4), calls=%async_computation | async-start | bytes 262144 | tf_op jit(solution)/shard_map/all_to_all | solution.py:108
  53.1 0.9 select_reduce_fusion.2
  54.0 1.1 %fusion.43 = f32[16,32]{1,0:T(8,128)S(1)} fusion(bf16[16,2048]{1,0:T(8,128)(2,1)S(1)} %add_convert_fusion, bf16[2048,32]{0,1:T(8,128)(2,1)} %param.29), kind=kOutput, calls=%fused_computation.87 | convolution fusion | flops 2097152 | bytes 198656 | tf_op jit(solution)/shard_map/dot_general | solution.py:69
  55.1 5.9 %all-to-all-done = bf16[16,1,2,2048]{3,2,1,0:T(2,128)(2,1)S(1)} async-done(((bf16[16,1,2,2048]{3,2,1,0:T(2,128)(2,1)}), bf16[16,1,2,2048]{3,2,1,0:T(2,128)(2,1)S(1)}, u32[]{:S(2)}, u32[]{:S(2)}) %all-to-all-start) | async-done | bytes 131104 | tf_op jit(solution)/shard_map/all_to_all | solution.py:108
  61.0 1.5 %convolution_bitcast_fusion.1 = f32[16,1,2,256]{3,0,2,1:T(8,128)S(1)} fusion(bf16[1,2048,256]{2,1,0:T(8,128)(2,1)} %param.31, bf16[16,1,2,2048]{3,2,1,0:T(2,128)(2,1)S(1)} %all-to-all-done), kind=kOutput, calls=%fused_computation.10 | convolution fusion | flops 33554432 | bytes 1212416 | tf_op jit(solution)/shard_map/secd,edf->secf/dot_general | solution.py:109
  62.5 2.0 %fusion = bf16[16,1,2,2048]{3,0,2,1:T(8,128)(2,1)S(1)} fusion(bf16[1,256,2048]{2,1,0:T(8,128)(2,1)S(1)} %copy-done.2, bf16[1,2048,256]{2,1,0:T(8,128)(2,1)} %param.32, bf16[16,1,2,2048]{3,2,1,0:T(2,128)(2,1)S(1)} %all-to-all-done, f32[16,1,2,256]{3,0,2,1:T(8,128)S(1)} %convolution_bitcast_fusion.1), kind=kOutput, calls=%fused_computation.4 | convolution fusion | flops 67223552 | bytes 2392064 | tf_op jit(solution)/shard_map/secf,efd->secd/dot_general | solution.py:114
  64.4 0.8 copy.55
  65.2 3.5 %all-to-all-start.1 = ((bf16[16,1,2,2048]{3,2,1,0:T(2,128)(2,1)}), bf16[16,1,2,2048]{3,2,1,0:T(2,128)(2,1)S(1)}, u32[]{:S(2)}, u32[]{:S(2)}) async-start(bf16[16,1,2,2048]{3,2,1,0:T(2,128)(2,1)} %copy.55), calls=%async_computation.1 | async-start | bytes 262144 | tf_op jit(solution)/shard_map/all_to_all | solution.py:121
  68.7 0.2 select_reduce_fusion.1
  68.9 7.6 %all-to-all-done.1 = bf16[16,1,2,2048]{3,2,1,0:T(2,128)(2,1)S(1)} async-done(((bf16[16,1,2,2048]{3,2,1,0:T(2,128)(2,1)}), bf16[16,1,2,2048]{3,2,1,0:T(2,128)(2,1)S(1)}, u32[]{:S(2)}, u32[]{:S(2)}) %all-to-all-start.1) | async-done | bytes 131104 | tf_op jit(solution)/shard_map/all_to_all | solution.py:121
  76.6 0.2 pad_maximum_fusion
  76.8 3.8 %all_to_all.15 = bf16[2,16,1,2,1024]{4,3,1,2,0:T(2,128)(2,1)S(1)} all-to-all(bf16[2,16,1,2,1024]{4,3,1,2,0:T(2,128)(2,1)S(1)} %pad_maximum_fusion), channel_id=1, replica_groups=mesh['ep'=16,'tp'=2] {'tp'}, dimensions={0} | all-to-all | bytes 262144 | tf_op jit(solution)/shard_map/all_to_all | solution.py:118
  80.6 0.1 copy.57
  80.7 0.1 reshape.149
  80.8 0.2 fusion.1
  81.0 0.1 fusion.32
  81.1 2.5 %all-reduce = (f32[16]{0:T(128)S(1)}, f32[16]{0:T(128)S(1)}) all-reduce(f32[16]{0:T(128)S(1)} %get-tuple-element.3, f32[16]{0:T(128)S(1)} %get-tuple-element.2), channel_id=1, replica_groups=mesh['ep'=16,'tp'=2] {'tp'}, use_global_device_ids=true, to_apply=%region_15.16 | all-reduce | flops 32 | bytes 256 | tf_op jit(solution)/shard_map/psum | solution.py:140
  83.6 0.7 add_convert_fusion.1
  (37 shorter events, 0.4 us)
Async XLA Ops:
  7.2 11.5 %copy-start = (bf16[512,2048]{1,0:T(8,128)(2,1)S(1)}, bf16[512,2048]{1,0:T(8,128)(2,1)}, u32[]{:S(2)}) copy-start(bf16[512,2048]{1,0:T(8,128)(2,1)} %param.25) | copy-start | bytes 6291460
  7.2 3.8 %copy-start.1 = (bf16[16,2048]{1,0:T(8,128)(2,1)S(1)}, bf16[16,2048]{1,0:T(8,128)(2,1)}, u32[]{:S(2)}) copy-start(bf16[16,2048]{1,0:T(8,128)(2,1)} %param.17) | copy-start | bytes 196612
  7.2 3.8 %copy-start.3 = (bf16[2048,256]{1,0:T(8,128)(2,1)S(1)}, bf16[2048,256]{1,0:T(8,128)(2,1)}, u32[]{:S(2)}) copy-start(bf16[2048,256]{1,0:T(8,128)(2,1)} %param.20) | copy-start | bytes 3145732
  7.2 35.1 %all-reduce.3.cloned.1.call-start = ((), (), s32[]{:S(2)}) async-start(), calls=%async_computation.3 | async-start | bytes 131072 | tf_op jit(solution)/shard_map/psum | solution.py:60
  12.8 5.9 %copy-start.7 = (f32[256]{0:T(256)S(1)}, f32[256]{0:T(256)}, u32[]{:S(2)}) copy-start(f32[256]{0:T(256)} %param.24) | copy-start | bytes 3076
  18.7 3.1 %copy-start.6 = (s32[16,2]{0,1:T(2,128)S(1)}, s32[16,2]{0,1:T(2,128)}, u32[]{:S(2)}) copy-start(s32[16,2]{0,1:T(2,128)} %param.30) | copy-start | bytes 388
  18.7 3.6 %copy-start.4 = (f32[2,2048]{1,0:T(2,128)S(1)}, f32[2,2048]{1,0:T(2,128)}, u32[]{:S(2)}) copy-start(f32[2,2048]{1,0:T(2,128)} %param.27) | copy-start | bytes 49156
  18.7 3.7 %copy-start.5 = (f32[2,2048]{1,0:T(2,128)S(1)}, f32[2,2048]{1,0:T(2,128)}, u32[]{:S(2)}) copy-start(f32[2,2048]{1,0:T(2,128)} %param.26) | copy-start | bytes 49156
  21.7 40.8 %copy-start.2 = (bf16[1,256,2048]{2,1,0:T(8,128)(2,1)S(1)}, bf16[1,256,2048]{2,1,0:T(8,128)(2,1)}, u32[]{:S(2)}) copy-start(bf16[1,256,2048]{2,1,0:T(8,128)(2,1)} %param.33) | copy-start | bytes 3145732
  46.3 14.7 %all-to-all-start = ((bf16[16,1,2,2048]{3,2,1,0:T(2,128)(2,1)}), bf16[16,1,2,2048]{3,2,1,0:T(2,128)(2,1)S(1)}, u32[]{:S(2)}, u32[]{:S(2)}) async-start(bf16[16,1,2,2048]{3,2,1,0:T(2,128)(2,1)} %bitcast.4), calls=%async_computation | async-start | bytes 262144 | tf_op jit(solution)/shard_map/all_to_all | solution.py:108
  65.2 11.3 %all-to-all-start.1 = ((bf16[16,1,2,2048]{3,2,1,0:T(2,128)(2,1)}), bf16[16,1,2,2048]{3,2,1,0:T(2,128)(2,1)S(1)}, u32[]{:S(2)}, u32[]{:S(2)}) async-start(bf16[16,1,2,2048]{3,2,1,0:T(2,128)(2,1)} %copy.55), calls=%async_computation.1 | async-start | bytes 262144 | tf_op jit(solution)/shard_map/all_to_all | solution.py:121
Sparse Core Ops, SparseCore 0:
  21.9 20.4 all-reduce.2
